TPU v7x, 32 devices: a whole 2x2x4 slice. The times are simulated.
32 devices in a mesh: grp: 2 (over x), kv: 4 (over z), tp: 4 (over y, core).
Axes of the slice: x: 2, y: 2, z: 4, core: 2. Of those that a mesh axis runs over, the one named last changes fastest.
Arguments:
- x_rows: bfloat16 [256, 4096], P('grp', 'kv'), parts along dimension 0, may hold values from -32 to 32
- in_gain: bfloat16 [4096], P('kv'), may hold values from 0.099609375 to 1.8984375
- query_weight: bfloat16 [4096, 4096], P('kv', 'tp'), may hold values from -0.09375 to 0.09375
- key_weight: bfloat16 [4096, 4096], P('kv', 'tp'), may hold values from -0.09375 to 0.09375
- value_weight: bfloat16 [4096, 8192], P('kv', 'tp'), may hold values from -0.09375 to 0.09375
- outgate_weight: bfloat16 [4096, 8192], P('kv', 'tp'), may hold values from -0.09375 to 0.09375
- input_gate_weight: bfloat16 [4096, 32], P('kv', 'tp'), may hold values from -0.09375 to 0.09375
- forget_gate_weight: bfloat16 [4096, 32], P('kv', 'tp'), may hold values from -0.09375 to 0.09375
- forget_bias: float32 [32], P('tp'), may hold values from -1 to 3
- state_matrix: float32 [256, 32, 128, 256], P(('grp', 'kv'), 'tp'), parts along dimension 0, may hold values from -3 to 3
- state_norm: float32 [256, 32, 128], P(('grp', 'kv'), 'tp'), parts along dimension 0, may hold values from -6 to 6
- state_max: float32 [256, 32], P(('grp', 'kv'), 'tp'), parts along dimension 0, may hold values from -1 to 1
- head_gain: bfloat16 [8192], P('tp'), may hold values from 0.099609375 to 1.8984375
- out_weight: bfloat16 [8192, 4096], P('tp', 'kv'), may hold values from -0.0625 to 0.0625
- mix_gain: bfloat16 [4096], P('kv'), may hold values from 0.099609375 to 1.8984375
- up_weight: bfloat16 [4096, 16384], P('kv', 'tp'), may hold values from -0.09375 to 0.09375
- down_weight: bfloat16 [16384, 4096], P('tp', 'kv'), may hold values from -0.046875 to 0.046875
Outputs:
- mixed_out: bfloat16 [256, 4096], P('grp', 'kv'), parts along dimension 0
- new_matrix: float32 [256, 32, 128, 256], P(('grp', 'kv'), 'tp'), parts along dimension 0
- new_norm: float32 [256, 32, 128], P(('grp', 'kv'), 'tp'), parts along dimension 0
- new_max: float32 [256, 32], P(('grp', 'kv'), 'tp'), parts along dimension 0
There are 2 independent parts, one for each index of `grp`. A program takes and returns all parts, laid end to end along the dimension named above; an argument that names none is the same for every part. Nothing has to cross between parts.
All inputs are finite; a program needn't handle non-finite values.
Results may differ from a plain program's by a relative error of at most 0.019.
Values may be sent and summed in bfloat16 or wider, within the bound.
A program may use at most 192 MiB of HBM per device.

v0:
```python
import jax
import jax.numpy as jnp
from jax import lax
from jax.sharding import PartitionSpec as P

D = 4096
DQK = 128
DV = 256


epsilon = 1e-06


def per_device(
    x_rows,
    in_gain,
    query_weight,
    key_weight,
    value_weight,
    outgate_weight,
    input_gate_weight,
    forget_gate_weight,
    forget_bias,
    state_matrix,
    state_norm,
    state_max,
    head_gain,
    out_weight,
    mix_gain,
    up_weight,
    down_weight,
):
    xfull = x_rows.astype(jnp.float32)
    partial_squares = jnp.sum(xfull * xfull, axis=1)
    scaled = (xfull * in_gain.astype(jnp.float32)).astype(jnp.bfloat16)
    gate_columns = jnp.concatenate([input_gate_weight, forget_gate_weight], axis=1)

    def product(weight):
        return jnp.dot(scaled, weight, preferred_element_type=jnp.float32)

    query_part, key_part, value_part, outgate_part, gate_part, squares = (
        lax.psum_scatter(product(query_weight), "kv", scatter_dimension=0, tiled=True),
        lax.psum_scatter(product(key_weight), "kv", scatter_dimension=0, tiled=True),
        lax.psum_scatter(product(value_weight), "kv", scatter_dimension=0, tiled=True),
        lax.psum_scatter(product(outgate_weight), "kv", scatter_dimension=0, tiled=True),
        lax.psum_scatter(product(gate_columns), "kv", scatter_dimension=0, tiled=True),
        lax.psum_scatter(partial_squares, "kv", scatter_dimension=0, tiled=True),
    )
    scale = lax.rsqrt(squares / D + epsilon)[:, None]
    row_count = state_max.shape[0]
    head_count = state_max.shape[1]

    def rounded(partial_value):
        return lax.optimization_barrier((partial_value * scale).astype(jnp.bfloat16)).astype(
            jnp.float32
        )

    query = rounded(query_part).reshape(row_count, head_count, DQK) * DQK ** (-0.5)
    keys = rounded(key_part).reshape(row_count, head_count, DQK)
    values = rounded(value_part).reshape(row_count, head_count, DV)
    outgate = rounded(outgate_part).reshape(row_count, head_count, DV)
    gates = gate_part * scale
    igate = gates[:, :head_count]
    fgate = gates[:, head_count:]
    log_forget = jax.nn.log_sigmoid(fgate + forget_bias[None, :])
    new_max = jnp.maximum(log_forget + state_max, igate)
    fdecay = jnp.exp(log_forget + state_max - new_max)
    idecay = jnp.exp(igate - new_max)
    new_matrix = fdecay[:, :, None, None] * state_matrix + idecay[:, :, None, None] * (
        keys[:, :, :, None] * values[:, :, None, :]
    )
    new_norm = fdecay[:, :, None] * state_norm + idecay[:, :, None] * keys
    numer = jnp.einsum("bhd,bhde->bhe", query, new_matrix, precision=lax.Precision.HIGHEST)
    denom = jnp.sum(query * new_norm, axis=-1)
    readout = numer / jnp.maximum(jnp.abs(denom), jnp.exp(-new_max))[:, :, None]
    normed = readout * lax.rsqrt(jnp.mean(readout * readout, axis=-1, keepdims=True) + epsilon)
    normed = normed * head_gain.astype(jnp.float32).reshape(head_count, DV)
    merged = (
        (jax.nn.sigmoid(outgate) * normed).reshape(row_count, head_count * DV).astype(jnp.bfloat16)
    )
    branch = jnp.dot(
        lax.all_gather(merged, "kv", axis=0, tiled=True),
        out_weight,
        preferred_element_type=jnp.float32,
    )
    branch = lax.psum(branch, "tp")
    resid = lax.optimization_barrier((xfull + branch).astype(jnp.bfloat16)).astype(jnp.float32)
    partial_two = jnp.sum(resid * resid, axis=1)
    scaled_two = (resid * mix_gain.astype(jnp.float32)).astype(jnp.bfloat16)
    up_part = jnp.dot(scaled_two, up_weight, preferred_element_type=jnp.float32)
    up_total, squares_two = (
        lax.psum_scatter(up_part, "kv", scatter_dimension=0, tiled=True),
        lax.psum_scatter(partial_two, "kv", scatter_dimension=0, tiled=True),
    )
    scale_two = lax.rsqrt(squares_two / D + epsilon)[:, None]
    hidden = jnp.square(jax.nn.relu(up_total * scale_two)).astype(jnp.bfloat16)
    down = jnp.dot(
        lax.all_gather(hidden, "kv", axis=0, tiled=True),
        down_weight,
        preferred_element_type=jnp.float32,
    )
    down = lax.psum(down.astype(jnp.bfloat16), "tp").astype(jnp.float32)
    mixed_out = (resid + down).astype(jnp.bfloat16)
    return (mixed_out, new_matrix, new_norm, new_max)


def solution(mesh):
    placed = (
        P("grp", "kv"),
        P("kv"),
        P("kv", "tp"),
        P("kv", "tp"),
        P("kv", "tp"),
        P("kv", "tp"),
        P("kv", "tp"),
        P("kv", "tp"),
        P("tp"),
        P(("grp", "kv"), "tp", None, None),
        P(("grp", "kv"), "tp", None),
        P(("grp", "kv"), "tp"),
        P("tp"),
        P("tp", "kv"),
        P("kv"),
        P("kv", "tp"),
        P("tp", "kv"),
    )
    return jax.shard_map(
        per_device,
        mesh=mesh,
        in_specs=placed,
        out_specs=(
            P("grp", "kv"),
            P(("grp", "kv"), "tp", None, None),
            P(("grp", "kv"), "tp", None),
            P(("grp", "kv"), "tp"),
        ),
        check_vma=False,
    )
```

profile of v0, /device:TPU:0, one launch (start us, length us, event | category | flops | bytes accessed | tf_op | source)
XLA Modules:
  0.0 355.6 jit_solution(17088462818694971066)
XLA Ops:
  7.2 0.0 copy-start
  7.2 0.0 copy-start.2
  7.2 0.0 reduce-scatter.19.cloned.1.call-start
  7.2 0.8 convert_element_type.61
  8.1 1.8 fusion.14
  9.9 0.0 reduce-scatter.19.cloned.1.call-update
  9.9 0.0 reduce-scatter.11.cloned.1.call-start
  10.0 2.2 fusion.16
  12.2 0.0 reduce-scatter.11.cloned.1.call-update
  12.2 0.0 copy-start.10
  12.3 0.0 reduce-scatter.13.cloned.1.call-start
  12.3 3.0 fusion.12
  15.3 0.0 reduce-scatter.13.cloned.1.call-update
  15.3 0.0 reduce-scatter.15.cloned.1.call-start
  15.3 4.0 %fusion.10 = f32[128,2048]{1,0:T(8,128)} fusion(bf16[1024,2048]{1,0:T(8,128)(2,1)} %param.21, bf16[128,1024]{1,0:T(8,128)(2,1)} %param.17, f32[1024]{0:T(1024)S(1)} %convert_element_type.61), kind=kOutput, calls=%fused_computation.30 | convolution fusion | flops 537264128 | bytes 5509120 | tf_op jit(solution)/shard_map/dot_general | solution.py:39
  19.3 0.0 reduce-scatter.15.cloned.1.call-update
  19.3 0.0 reduce-scatter.9.cloned.1.call-start
  19.4 3.9 %fusion.18 = f32[128,2048]{1,0:T(8,128)} fusion(bf16[1024,2048]{1,0:T(8,128)(2,1)} %param.22, bf16[128,1024]{1,0:T(8,128)(2,1)S(1)} %copy-done.2, f32[1024]{0:T(1024)S(1)} %convert_element_type.61), kind=kOutput, calls=%fused_computation.34 | convolution fusion | flops 537264128 | bytes 5509120 | tf_op jit(solution)/shard_map/dot_general | solution.py:39
  23.3 0.0 reduce-scatter.9.cloned.1.call-update
  23.3 0.0 all-reduce.5.cloned.1.call-start
  23.4 0.1 fusion.1
  23.5 0.6 dynamic-slice
  24.8 0.1 copy.27
  24.9 13.4 %all-reduce = f32[128]{0:T(128)S(1)} all-reduce(f32[128]{0:T(128)S(1)} %fusion.1), channel_id=3, replica_groups=mesh['grp'=2,'kv'=4,'tp'=4] {'kv'}, use_global_device_ids=true, to_apply=%region_2.0.clone | all-reduce | flops 128 | bytes 1024
  38.3 0.1 fusion.28
  38.4 0.8 broadcast_multiply_fusion
  39.2 0.1 subtract_exponential_fusion.1
  39.3 15.9 %reduce-scatter.11.cloned.1.call-done = f32[32,1024]{1,0:T(8,128)} async-done(((f32[128,1024]{1,0:T(8,128)}), f32[32,1024]{1,0:T(8,128)}) %reduce-scatter.11.cloned.1.call-update) | async-done | bytes 131088 | tf_op jit(solution)/shard_map/reduce_scatter | solution.py:42
  55.2 22.4 %reduce-scatter.13.cloned.1.call-done = f32[32,1024]{1,0:T(8,128)} async-done(((f32[128,1024]{1,0:T(8,128)}), f32[32,1024]{1,0:T(8,128)}) %reduce-scatter.13.cloned.1.call-update) | async-done | bytes 131088 | tf_op jit(solution)/shard_map/reduce_scatter | solution.py:43
  77.6 1.1 multiply_convert_fusion.3
  78.8 0.1 multiply_add_fusion.1
  78.9 0.0 copy-start.4
  79.0 0.1 multiply_reduce_fusion.1
  79.1 26.9 %reduce-scatter.15.cloned.1.call-done = f32[32,2048]{1,0:T(8,128)} async-done(((f32[128,2048]{1,0:T(8,128)}), f32[32,2048]{1,0:T(8,128)}) %reduce-scatter.15.cloned.1.call-update) | async-done | bytes 262160 | tf_op jit(solution)/shard_map/reduce_scatter | solution.py:44
  105.9 27.9 %reduce-scatter.9.cloned.1.call-done = f32[32,2048]{1,0:T(8,128)} async-done(((f32[128,2048]{1,0:T(8,128)}), f32[32,2048]{1,0:T(8,128)}) %reduce-scatter.9.cloned.1.call-update) | async-done | bytes 262160 | tf_op jit(solution)/shard_map/reduce_scatter | solution.py:45
  133.9 1.1 multiply_convert_fusion.1
  135.0 0.1 add_divide_fusion
  135.1 0.1 copy.33
  135.2 24.5 %multiply_add_fusion = f32[32,8,128,256]{3,2,1,0:T(8,128)} fusion(f32[32,8,128,256]{3,2,1,0:T(8,128)} %param.26, f32[32,8,256]{2,1,0:T(8,128)S(1)} %bitcast.45, f32[32,8,128]{2,1,0:T(8,128)S(1)} %bitcast.44, f32[32,8]{1,0:T(8,128)S(1)} %subtract_exponential_fusion, f32[32,8]{1,0:T(8,128)S(1)} %get-tuple-element.8), kind=kLoop, calls=%fused_computation | loop fusion | flops 33554432 | bytes 67504128 | tf_op jit(solution)/shard_map/add | solution.py:69
  159.8 19.8 %fusion.31 = f32[32,8,1,256]{3,2,1,0:T(1,128)S(1)} fusion(f32[32,8,128,1]{2,3,1,0:T(1,128)S(1)} %bitcast.43, f32[32,8,128,256]{3,2,1,0:T(8,128)} %multiply_add_fusion), kind=kOutput, calls=%fused_computation.56 | convolution fusion | flops 100663296 | bytes 33947648 | tf_op jit(solution)/shard_map/bhd,bhde->bhe/dot_general | solution.py:73
  179.6 0.2 multiply_reduce_fusion
  179.8 0.1 fusion.8
  179.9 16.0 %all_gather.6 = bf16[128,2048]{1,0:T(8,128)(2,1)S(1)} all-gather(bf16[32,2048]{1,0:T(8,128)(2,1)S(1)} %bitcast.47), channel_id=1, replica_groups=mesh['grp'=2,'kv'=4,'tp'=4] {'kv'}, dimensions={0}, use_global_device_ids=true | all-gather | bytes 655360 | tf_op jit(solution)/shard_map/all_gather | solution.py:82
  195.9 1.6 fusion.32
  197.4 0.0 all-reduce.5.cloned.1.call-update
  197.5 0.0 reduce-scatter.17.cloned.1.call-start
  197.5 31.9 %all-reduce.5.cloned.1.call-done = f32[128,1024]{1,0:T(8,128)} async-done(((f32[128,1024]{1,0:T(8,128)}), f32[128,1024]{1,0:T(8,128)}) %all-reduce.5.cloned.1.call-update) | async-done | bytes 524304 | tf_op jit(solution)/shard_map/psum | solution.py:86
  229.4 1.1 fusion.2
  230.5 6.0 %fusion.6 = f32[128,4096]{1,0:T(8,128)} fusion(bf16[1024,4096]{1,0:T(8,128)(2,1)} %param.32, bf16[128,1024]{1,0:T(8,128)(2,1)S(1)} %fusion.2, f32[1024]{0:T(1024)S(1)} %convert_element_type.73), kind=kOutput, calls=%fused_computation.15 | convolution fusion | flops 1074135040 | bytes 10752000 | tf_op jit(solution)/shard_map/dot_general | solution.py:90
  236.5 0.0 reduce-scatter.17.cloned.1.call-update
  236.5 0.0 all-gather.2.cloned.1.call-start
  236.6 0.1 fusion.4
  236.7 11.8 %all-reduce.1 = f32[128]{0:T(128)S(1)} all-reduce(f32[128]{0:T(128)S(1)} %fusion.4), channel_id=9, replica_groups=mesh['grp'=2,'kv'=4,'tp'=4] {'kv'}, use_global_device_ids=true, to_apply=%region_12.13.clone | all-reduce | flops 128 | bytes 1024
  248.6 0.1 fusion.29
  248.6 31.8 %reduce-scatter.17.cloned.1.call-done = f32[32,4096]{1,0:T(8,128)} async-done(((f32[128,4096]{1,0:T(8,128)}), f32[32,4096]{1,0:T(8,128)}) %reduce-scatter.17.cloned.1.call-update) | async-done | bytes 524304 | tf_op jit(solution)/shard_map/reduce_scatter | solution.py:92
  280.5 1.9 multiply_convert_fusion
  282.3 0.0 all-gather.2.cloned.1.call-update
  282.4 0.0 all-reduce.7.cloned.1.call-start
  282.4 27.4 %all-gather.2.cloned.1.call-done = bf16[128,4096]{1,0:T(8,128)(2,1)} async-done(((bf16[32,4096]{1,0:T(8,128)(2,1)}), bf16[128,4096]{1,0:T(8,128)(2,1)}) %all-gather.2.cloned.1.call-update) | async-done | bytes 1048592 | tf_op jit(solution)/shard_map/all_gather | solution.py:98
  309.8 5.7 %convolution_convert_fusion = bf16[128,1024]{1,0:T(8,128)(2,1)} fusion(bf16[128,4096]{1,0:T(8,128)(2,1)} %all-gather.2.cloned.1.call-done, bf16[4096,1024]{1,0:T(8,128)(2,1)} %param.33), kind=kOutput, calls=%fused_computation.1 | convolution fusion | flops 1073872896 | bytes 9699328 | tf_op jit(solution)/shard_map/dot_general | solution.py:97
  315.5 0.0 all-reduce.7.cloned.1.call-update
  315.5 0.7 copy.28
  316.2 31.2 %all-reduce.7.cloned.1.call-done = bf16[128,1024]{1,0:T(8,128)(2,1)} async-done(((bf16[128,1024]{1,0:T(8,128)(2,1)}), bf16[128,1024]{1,0:T(8,128)(2,1)}) %all-reduce.7.cloned.1.call-update) | async-done | bytes 262160 | tf_op jit(solution)/shard_map/psum | solution.py:102
  347.3 1.7 fusion.5
  (30 shorter events, 0.2 us)
Async XLA Ops:
  7.2 2.8 copy-start
  7.2 12.2 %copy-start.2 = (bf16[128,1024]{1,0:T(8,128)(2,1)S(1)}, bf16[128,1024]{1,0:T(8,128)(2,1)}, u32[]{:S(2)}) copy-start(bf16[128,1024]{1,0:T(8,128)(2,1)} %param.17) | copy-start | bytes 786436
  7.2 31.2 %reduce-scatter.19.cloned.1.call-start = ((), (), s32[]{:S(2)}) async-start(), calls=%async_computation.14 | async-start | bytes 81920 | tf_op jit(solution)/shard_map/reduce_scatter | solution.py:46
  9.9 45.3 %reduce-scatter.11.cloned.1.call-start = ((), (), s32[]{:S(2)}) async-start(), calls=%async_computation.7 | async-start | bytes 655360 | tf_op jit(solution)/shard_map/reduce_scatter | solution.py:42
  12.2 11.3 %copy-start.10 = (u32[32]{0:T(128)S(1)}, u32[32]{0:T(128)}, u32[]{:S(2)}) copy-start(u32[32]{0:T(128)} %constant.23) | copy-start | bytes 388
  12.2 12.5 %copy-start.6 = (bf16[2048]{0:T(1024)(128)(2,1)S(1)}, bf16[2048]{0:T(1024)(128)(2,1)}, u32[]{:S(2)}) copy-start(bf16[2048]{0:T(1024)(128)(2,1)} %param.29) | copy-start | bytes 12292
  12.2 12.6 %copy-start.7 = (f32[32,8]{0,1:T(8,128)S(1)}, f32[32,8]{0,1:T(8,128)}, u32[]{:S(2)}) copy-start(f32[32,8]{0,1:T(8,128)} %param.28) | copy-start | bytes 3076
  12.2 26.9 %copy-start.9 = (f32[8]{0:T(128)S(1)}, f32[8]{0:T(128)}, u32[]{:S(2)}) copy-start(f32[8]{0:T(128)} %param.25) | copy-start | bytes 100
  12.3 65.4 %reduce-scatter.13.cloned.1.call-start = ((), (), s32[]{:S(2)}) async-start(), calls=%async_computation.8 | async-start | bytes 655360 | tf_op jit(solution)/shard_map/reduce_scatter | solution.py:43
  15.3 63.5 %copy-start.5 = (f32[32,8,128]{2,1,0:T(8,128)S(1)}, f32[32,8,128]{2,1,0:T(8,128)}, u32[]{:S(2)}) copy-start(f32[32,8,128]{2,1,0:T(8,128)} %param.27) | copy-start | bytes 393220
  15.3 90.7 %reduce-scatter.15.cloned.1.call-start = ((), (), s32[]{:S(2)}) async-start(), calls=%async_computation.9 | async-start | bytes 1310720 | tf_op jit(solution)/shard_map/reduce_scatter | solution.py:44
  19.3 114.6 %reduce-scatter.9.cloned.1.call-start = ((), (), s32[]{:S(2)}) async-start(), calls=%async_computation.6 | async-start | bytes 1310720 | tf_op jit(solution)/shard_map/reduce_scatter | solution.py:45
  23.3 206.1 %all-reduce.5.cloned.1.call-start = ((), (), s32[]{:S(2)}) async-start(), calls=%async_computation.10 | async-start | bytes 1048576 | tf_op jit(solution)/shard_map/psum | solution.py:86
  78.9 80.8 %copy-start.4 = (f32[32,8,128]{2,1,0:T(8,128)}, f32[32,8,128]{2,1,0:T(8,128)S(1)}, u32[]{:S(2)}) copy-start(f32[32,8,128]{2,1,0:T(8,128)S(1)} %multiply_add_fusion.1) | copy-start | bytes 393220
  159.7 36.1 %copy-start.3 = (bf16[2048,1024]{1,0:T(8,128)(2,1)S(1)}, bf16[2048,1024]{1,0:T(8,128)(2,1)}, u32[]{:S(2)}) copy-start(bf16[2048,1024]{1,0:T(8,128)(2,1)} %param.30) | copy-start | bytes 12582916
  159.7 37.8 %copy-start.8 = (bf16[1024]{0:T(1024)(128)(2,1)S(1)}, bf16[1024]{0:T(1024)(128)(2,1)}, u32[]{:S(2)}) copy-start(bf16[1024]{0:T(1024)(128)(2,1)} %param.31) | copy-start | bytes 6148
  197.5 83.0 %reduce-scatter.17.cloned.1.call-start = ((), (), s32[]{:S(2)}) async-start(), calls=%async_computation.11 | async-start | bytes 2621440 | tf_op jit(solution)/shard_map/reduce_scatter | solution.py:92
  236.5 73.3 %all-gather.2.cloned.1.call-start = ((), (), s32[]{:S(2)}) async-start(), calls=%async_computation.12 | async-start | bytes 1310720 | tf_op jit(solution)/shard_map/all_gather | solution.py:98
  282.4 66.7 %copy-start.1 = (bf16[1024,1024]{1,0:T(8,128)(2,1)S(1)}, bf16[1024,1024]{1,0:T(8,128)(2,1)}, u32[]{:S(2)}) copy-start(bf16[1024,1024]{1,0:T(8,128)(2,1)} %param.19) | copy-start | bytes 6291460
  282.4 65.0 %all-reduce.7.cloned.1.call-start = ((), (), s32[]{:S(2)}) async-start(), calls=%async_computation.13 | async-start | bytes 524288 | tf_op jit(solution)/shard_map/psum | solution.py:102
Sparse Core Ops, SparseCore 0:
  10.8 22.0 reduce-scatter.18
  35.2 19.9 reduce-scatter.10
  57.5 20.1 reduce-scatter.12
  80.3 25.5 reduce-scatter.14
  108.1 25.7 reduce-scatter.8
  197.6 31.7 all-reduce.4
  236.6 43.7 reduce-scatter.16
  282.6 27.1 all-gather.1
  315.6 31.6 all-reduce.6
where the time goes:
time: 356 us
  waiting for transfers between devices  216 us (61%)
  matrix products  47.9 us (13%)
  blocking collectives  41.2 us (12%)
  other arithmetic  34.2 us (10%)
  between operations  14.8 us (4%)
    psum x1, waiting for transfers between devices, per_device(): branch = lax.psum(branch, 'tp')  31.9 us
    reduce_scatter x1, waiting for transfers between devices, per_device(): lax.psum_scatter(up_part, 'kv', scatter_dimension=0, tiled=True)  31.8 us
    psum x1, waiting for transfers between devices, per_device(): down = lax.psum(down.astype(jnp.bfloat16), 'tp').astype(jnp.float32)  31.2 us
    reduce_scatter x1, waiting for transfers between devices, per_device(): lax.psum_scatter(product(outgate_weight), 'kv', scatter_dimension=0, tile...  27.9 us
    all_gather x1, waiting for transfers between devices, per_device(): lax.all_gather(hidden, 'kv', axis=0, tiled=True)  27.4 us
    reduce_scatter x1, waiting for transfers between devices, per_device(): lax.psum_scatter(product(value_weight), 'kv', scatter_dimension=0, tiled=...  26.9 us
    unnamed x2, blocking collectives  25.3 us
    add x1, other arithmetic, per_device(): fdecay[:, :, None, None] * state_matrix  24.5 us
  transfers between devices with their start and end apart: 9, of which 8 were waited for; matrix products, arithmetic and copies ran while one was open for 5% of the time, Pallas kernels for 0%

commit v1 on v0

v1 whole, which is shorter than its diff:
```python
import functools
import math

import jax
import jax.numpy as jnp
from jax import lax
from jax.experimental import pallas as pl
from jax.experimental.pallas import tpu as pltpu
from jax.sharding import PartitionSpec as P

LANES = 128
EPS = 1e-06
MESH = pl.DeviceIdType.MESH
F32 = jnp.float32
BF16 = jnp.bfloat16


def kernel(
    kvn,
    tpn,
    width,
    model,
    x_ref,
    x3_ref,
    gain_ref,
    q_hbm,
    k_hbm,
    v_hbm,
    o_hbm,
    gate_ref,
    bias_ref,
    state_hbm,
    norm_ref,
    max_ref,
    head_gain_ref,
    out_hbm,
    mix_gain_ref,
    up_hbm,
    down_hbm,
    mixed_ref,
    matrix_hbm,
    new_norm_ref,
    new_max_ref,
    weights,
    down_w,
    state,
    scaled,
    part,
    gate_send,
    gate_recv,
    proj_send,
    proj_recv,
    q_all,
    k_all,
    v_all,
    o_all,
    fd_all,
    id_all,
    em_all,
    merged,
    merged_all,
    branch_send,
    branch_recv,
    resid_all,
    sq_send,
    sq_recv,
    up_send,
    up_recv,
    hidden_all,
    mix_send,
    mix_recv,
    mixed_all,
    w_sem,
    w2_sem,
    down_sem,
    state_sem,
    write_sem,
    gate_ss,
    gate_rs,
    proj_ss,
    proj_rs,
    mg_ss,
    mg_rs,
    br_ss,
    br_rs,
    rd_ss,
    rd_rs,
    sq_ss,
    sq_rs,
    up_ss,
    up_rs,
    hd_ss,
    hd_rs,
    mx_ss,
    mx_rs,
    ma_ss,
    ma_rs,
):
    me = lax.axis_index("kv")
    tme = lax.axis_index("tp")
    total, local = x_ref.shape
    rows, heads, dqk = norm_ref.shape
    dv = head_gain_ref.shape[1]
    trows = total // tpn
    tile = min(256, width)
    hidden_units = up_hbm.shape[1]

    def kv_peer(j):
        return lax.rem(me + j, kvn)

    def tp_peer(j):
        return lax.rem(tme + j, tpn)

    def send(src, dst, ssem, rsem, axis, peer):
        copy = pltpu.make_async_remote_copy(
            src_ref=src,
            dst_ref=dst,
            send_sem=ssem,
            recv_sem=rsem,
            device_id={axis: peer},
            device_id_type=MESH,
        )
        copy.start()
        return copy

    sent = []

    first = []
    for name, ref in enumerate((q_hbm, k_hbm, v_hbm, o_hbm)):
        for offset in range(0, ref.shape[1], width):
            first.append((name, ref, offset))
    loads = []
    for c, (name, ref, offset) in enumerate(first):
        copy = pltpu.make_async_copy(
            ref.at[:, pl.ds(offset, width)], weights.at[c], w_sem.at[c]
        )
        copy.start()
        loads.append(copy)
    second = []
    for a in range(0, out_hbm.shape[0], local):
        for b in range(0, out_hbm.shape[1], width):
            second.append((out_hbm, a, b))
    out_blocks = len(second)
    for b in range(0, hidden_units, width):
        second.append((up_hbm, 0, b))

    barrier = pltpu.get_barrier_semaphore()
    for j in range(1, kvn):
        pl.semaphore_signal(barrier, inc=1, device_id={"kv": kv_peer(j)}, device_id_type=MESH)
    for j in range(1, tpn):
        pl.semaphore_signal(barrier, inc=1, device_id={"tp": tp_peer(j)}, device_id_type=MESH)

    xf = x_ref[...].astype(F32)
    squares = jnp.sum(xf * xf, axis=1, keepdims=True)
    scaled[...] = (xf * gain_ref[...].astype(F32)).astype(BF16)
    gates = jnp.dot(scaled[...], gate_ref[...], preferred_element_type=F32)
    gate_send[:, :, 0 : 2 * LANES] = gates.reshape(kvn, rows, 2 * LANES)
    gate_send[:, :, 2 * LANES :] = jnp.broadcast_to(squares, (total, LANES)).reshape(
        kvn, rows, LANES
    )
    pl.semaphore_wait(barrier, (kvn - 1) + (tpn - 1))
    gate_copies = []
    for j in range(1, kvn):
        gate_copies.append(
            send(gate_send.at[kv_peer(j)], gate_recv.at[j - 1], gate_ss.at[j - 1], gate_rs.at[j - 1], "kv", kv_peer(j))
        )
    sent += gate_copies

    def matmul_chunk(lhs, slot, dest, c):
        def body(i, carry):
            cols = pl.ds(pl.multiple_of(i * tile, tile), tile)
            res = jnp.dot(lhs[...], weights[slot, :, cols], preferred_element_type=F32)
            dest[c, :, :, cols] = res.reshape(kvn, rows, tile).astype(BF16)
            return carry

        lax.fori_loop(0, width // tile, body, 0)

    def state_load(r):
        return pltpu.make_async_copy(state_hbm.at[r], state.at[r], state_sem.at[r])

    def state_store(r):
        return pltpu.make_async_copy(state.at[r], matrix_hbm.at[r], write_sem.at[r])

    proj_copies = []
    loads2 = []
    for c in range(len(first)):
        loads[c].wait()
        matmul_chunk(scaled, c, proj_send, c)
        for j in range(1, kvn):
            proj_copies.append(
                send(
                    proj_send.at[c, kv_peer(j)],
                    proj_recv.at[c, j - 1],
                    proj_ss.at[c, j - 1],
                    proj_rs.at[c, j - 1],
                    "kv",
                    kv_peer(j),
                )
            )
    sent += proj_copies
    for r in range(rows):
        state_load(r).start()
    for c, (ref, a, b) in enumerate(second):
        copy = pltpu.make_async_copy(
            ref.at[pl.ds(a, local), pl.ds(b, width)], weights.at[c], w2_sem.at[c]
        )
        copy.start()
        loads2.append(copy)
    down_load = pltpu.make_async_copy(down_hbm, down_w, down_sem.at[0])
    down_load.start()

    for copy in gate_copies:
        copy.wait_recv()
    gsum = gate_send[me]
    for j in range(1, kvn):
        gsum = gsum + gate_recv[j - 1]
    scale = lax.rsqrt(gsum[:, 2 * LANES : 2 * LANES + 1] / model + EPS)
    igate = gsum[:, 0:heads] * scale
    z = gsum[:, LANES : LANES + heads] * scale + bias_ref[...]
    logf = jnp.minimum(z, 0.0) - jnp.log1p(jnp.exp(-jnp.abs(z)))
    held = logf + max_ref[...]
    new_max = jnp.maximum(held, igate)
    new_max_ref[...] = new_max
    fdec = jnp.exp(held - new_max)
    idec = jnp.exp(igate - new_max)
    floor = jnp.exp(-new_max)
    for h in range(heads):
        for src, dst in ((fdec, fd_all), (idec, id_all), (floor, em_all)):
            dst[:, h, :] = jnp.broadcast_to(src[:, h : h + 1], (rows, LANES))

    targets = ((q_all, dqk), (k_all, dqk), (v_all, dv), (o_all, dv))
    for c, (name, ref, offset) in enumerate(first):
        for j in range(1, kvn):
            proj_copies[c * (kvn - 1) + j - 1].wait_recv()
        dst, extent = targets[name]
        for g in range(0, width, LANES):
            val = proj_send[c, me, :, g : g + LANES].astype(F32)
            for j in range(1, kvn):
                val = val + proj_recv[c, j - 1, :, g : g + LANES].astype(F32)
            val = (val * scale).astype(BF16).astype(F32)
            if name == 0:
                val = val * (dqk ** (-0.5))
            at = offset + g
            col = at % extent
            dst[:, at // extent, col : col + LANES] = val

    pad = jnp.zeros((LANES - 2 * heads, dqk), F32)

    def row_body(r, carry):
        state_load(r).wait()
        q8, k8, v8, o8 = q_all[r], k_all[r], v_all[r], o_all[r]
        fd8, id8, em8 = fd_all[r], id_all[r], em_all[r]
        ik8 = id8 * k8
        turned = jnp.concatenate([ik8, q8, pad], axis=0).T
        numer = []
        for h in range(heads):
            fd = jnp.concatenate([fd8[h : h + 1, :]] * (dv // LANES), axis=1)
            new = fd * state[r, h] + turned[:, h : h + 1] * v8[h : h + 1, :]
            state[r, h] = new
            numer.append(
                jnp.sum(turned[:, heads + h : heads + h + 1] * new, axis=0, keepdims=True)
            )
        state_store(r).start()
        numer = jnp.concatenate(numer, axis=0)
        nn = fd8 * norm_ref[r] + ik8
        new_norm_ref[r] = nn
        denom = jnp.sum(q8 * nn, axis=1, keepdims=True)
        readout = numer / jnp.maximum(jnp.abs(denom), em8[:, 0:1])
        normed = readout * lax.rsqrt(
            jnp.sum(readout * readout, axis=1, keepdims=True) / dv + EPS
        )
        merged[r] = jax.nn.sigmoid(o8) * (normed * head_gain_ref[...])
        return carry

    lax.fori_loop(0, rows, row_body, 0)

    for h in range(heads):
        merged_all[me, :, h * dv : (h + 1) * dv] = merged[:, h, :].astype(BF16)
    mg = []
    for j in range(1, kvn):
        mg.append(
            send(merged_all.at[me], merged_all.at[me], mg_ss.at[j - 1], mg_rs.at[j - 1], "kv", kv_peer(j))
        )
    sent += mg
    for c in range(out_blocks):
        loads2[c].wait()
    for copy in mg:
        copy.wait_recv()
    for b in range(0, local, width):

        def out_body(i, carry, b=b):
            cols = pl.ds(pl.multiple_of(i * tile, tile), tile)
            acc = jnp.zeros((total, tile), F32)
            for c in range(out_blocks):
                _, a, bb = second[c]
                if bb != b:
                    continue
                lhs = merged_all[:, :, a : a + local].reshape(total, local)
                acc = acc + jnp.dot(lhs, weights[c, :, cols], preferred_element_type=F32)
            part[:, pl.ds(pl.multiple_of(b + i * tile, tile), tile)] = acc
            return carry

        lax.fori_loop(0, width // tile, out_body, 0)

    def reduce_tp(buf_send, buf_recv, ssem, rsem):
        for j in range(tpn):
            buf_send[j] = part[j * trows : (j + 1) * trows, :].astype(BF16)
        copies = []
        for j in range(1, tpn):
            copies.append(
                send(buf_send.at[tp_peer(j)], buf_recv.at[j - 1], ssem.at[j - 1], rsem.at[j - 1], "tp", tp_peer(j))
            )
        for copy in copies:
            copy.wait_recv()
        val = buf_send[tme].astype(F32)
        for j in range(1, tpn):
            val = val + buf_recv[j - 1].astype(F32)
        return val, copies

    def gather_tp(buf, ssem, rsem):
        copies = []
        for j in range(1, tpn):
            copies.append(
                send(buf.at[tme], buf.at[tme], ssem.at[j - 1], rsem.at[j - 1], "tp", tp_peer(j))
            )
        for copy in copies:
            copy.wait_recv()
        return copies

    branch, copies = reduce_tp(branch_send, branch_recv, br_ss, br_rs)
    sent += copies
    resid_all[tme] = (x3_ref[tme].astype(F32) + branch).astype(BF16)
    sent += gather_tp(resid_all, rd_ss, rd_rs)

    for j in range(tpn):
        part[j * trows : (j + 1) * trows, :] = resid_all[j].astype(F32)
    rf = part[...]
    sq = jnp.sum(rf * rf, axis=1, keepdims=True)
    scaled[...] = (rf * mix_gain_ref[...].astype(F32)).astype(BF16)
    sq_send[...] = jnp.broadcast_to(sq, (total, LANES)).reshape(kvn, rows, LANES)
    sq_copies = []
    for j in range(1, kvn):
        sq_copies.append(
            send(sq_send.at[kv_peer(j)], sq_recv.at[j - 1], sq_ss.at[j - 1], sq_rs.at[j - 1], "kv", kv_peer(j))
        )
    sent += sq_copies
    chunks = hidden_units // width
    up_copies = []
    for c in range(chunks):
        loads2[out_blocks + c].wait()
        matmul_chunk(scaled, out_blocks + c, up_send, c)
        for j in range(1, kvn):
            up_copies.append(
                send(
                    up_send.at[c, kv_peer(j)],
                    up_recv.at[c, j - 1],
                    up_ss.at[c, j - 1],
                    up_rs.at[c, j - 1],
                    "kv",
                    kv_peer(j),
                )
            )
    sent += up_copies
    for copy in sq_copies:
        copy.wait_recv()
    sq_sum = sq_send[me]
    for j in range(1, kvn):
        sq_sum = sq_sum + sq_recv[j - 1]
    scale_two = lax.rsqrt(sq_sum[:, 0:1] / model + EPS)
    hidden_copies = []
    for c in range(chunks):
        for j in range(1, kvn):
            up_copies[c * (kvn - 1) + j - 1].wait_recv()
        val = up_send[c, me].astype(F32)
        for j in range(1, kvn):
            val = val + up_recv[c, j - 1].astype(F32)
        act = jnp.maximum(val * scale_two, 0.0)
        hidden_all[c, me] = (act * act).astype(BF16)
        for j in range(1, kvn):
            hidden_copies.append(
                send(
                    hidden_all.at[c, me],
                    hidden_all.at[c, me],
                    hd_ss.at[c, j - 1],
                    hd_rs.at[c, j - 1],
                    "kv",
                    kv_peer(j),
                )
            )
    sent += hidden_copies
    down_load.wait()
    for c in range(chunks):
        for j in range(1, kvn):
            hidden_copies[c * (kvn - 1) + j - 1].wait_recv()

        def down_body(i, carry, c=c):
            cols = pl.ds(pl.multiple_of(i * tile, tile), tile)
            lhs = hidden_all[c].reshape(total, width)
            res = jnp.dot(
                lhs, down_w[c * width : (c + 1) * width, cols], preferred_element_type=F32
            )
            if c == 0:
                part[:, cols] = res
            else:
                part[:, cols] += res
            return carry

        lax.fori_loop(0, local // tile, down_body, 0)
    down, copies = reduce_tp(mix_send, mix_recv, mx_ss, mx_rs)
    sent += copies
    mixed_all[tme] = (resid_all[tme].astype(F32) + down).astype(BF16)
    sent += gather_tp(mixed_all, ma_ss, ma_rs)
    mixed_ref[...] = mixed_all[...]

    for copy in sent:
        copy.wait_send()

    def drain(r, carry):
        state_store(r).wait()
        return carry

    lax.fori_loop(0, rows, drain, 0)


def per_device(
    kvn,
    tpn,
    x_rows,
    in_gain,
    query_weight,
    key_weight,
    value_weight,
    outgate_weight,
    input_gate_weight,
    forget_gate_weight,
    forget_bias,
    state_matrix,
    state_norm,
    state_max,
    head_gain,
    out_weight,
    mix_gain,
    up_weight,
    down_weight,
):
    total, local = x_rows.shape
    rows, heads, dqk, dv = state_matrix.shape
    trows = total // tpn
    hidden_units = up_weight.shape[1]
    width = functools.reduce(
        math.gcd,
        [local, heads * dqk, heads * dv, hidden_units],
    )
    n_first = (2 * heads * dqk + 2 * heads * dv) // width
    n_second = (heads * dv // local) * (local // width) + hidden_units // width
    chunks = hidden_units // width
    gap = ((0, 0), (0, LANES - heads))
    gate = jnp.concatenate(
        [jnp.pad(input_gate_weight, gap), jnp.pad(forget_gate_weight, gap)], axis=1
    )
    vmem = pl.BlockSpec(memory_space=pltpu.VMEM)
    hbm = pl.BlockSpec(memory_space=pl.ANY)
    V = pltpu.VMEM
    dma = pltpu.SemaphoreType.DMA
    k1, t1 = max(kvn - 1, 1), max(tpn - 1, 1)
    scratch = [
        V((max(n_first, n_second), local, width), BF16),
        V((hidden_units, local), BF16),
        V((rows, heads, dqk, dv), F32),
        V((total, local), BF16),
        V((total, local), F32),
        V((kvn, rows, 3 * LANES), F32),
        V((k1, rows, 3 * LANES), F32),
        V((n_first, kvn, rows, width), BF16),
        V((n_first, k1, rows, width), BF16),
        V((rows, heads, dqk), F32),
        V((rows, heads, dqk), F32),
        V((rows, heads, dv), F32),
        V((rows, heads, dv), F32),
        V((rows, heads, LANES), F32),
        V((rows, heads, LANES), F32),
        V((rows, heads, LANES), F32),
        V((rows, heads, dv), F32),
        V((kvn, rows, heads * dv), BF16),
        V((tpn, trows, local), BF16),
        V((t1, trows, local), BF16),
        V((tpn, trows, local), BF16),
        V((kvn, rows, LANES), F32),
        V((k1, rows, LANES), F32),
        V((chunks, kvn, rows, width), BF16),
        V((chunks, k1, rows, width), BF16),
        V((chunks, kvn, rows, width), BF16),
        V((tpn, trows, local), BF16),
        V((t1, trows, local), BF16),
        V((tpn, trows, local), BF16),
        dma((n_first,)),
        dma((n_second,)),
        dma((1,)),
        dma((rows,)),
        dma((rows,)),
        dma((k1,)),
        dma((k1,)),
        dma((n_first, k1)),
        dma((n_first, k1)),
        dma((k1,)),
        dma((k1,)),
        dma((t1,)),
        dma((t1,)),
        dma((t1,)),
        dma((t1,)),
        dma((k1,)),
        dma((k1,)),
        dma((chunks, k1)),
        dma((chunks, k1)),
        dma((chunks, k1)),
        dma((chunks, k1)),
        dma((t1,)),
        dma((t1,)),
        dma((t1,)),
        dma((t1,)),
    ]
    model = local * kvn
    mixed, new_matrix, new_norm, new_max = pl.pallas_call(
        functools.partial(kernel, kvn, tpn, width, model),
        out_shape=(
            jax.ShapeDtypeStruct((tpn, trows, local), BF16),
            jax.ShapeDtypeStruct(state_matrix.shape, F32),
            jax.ShapeDtypeStruct(state_norm.shape, F32),
            jax.ShapeDtypeStruct(state_max.shape, F32),
        ),
        in_specs=[vmem, vmem, vmem, hbm, hbm, hbm, hbm, vmem, vmem, hbm, vmem, vmem, vmem, hbm, vmem, hbm, hbm],
        out_specs=(vmem, hbm, vmem, vmem),
        scratch_shapes=scratch,
        compiler_params=pltpu.CompilerParams(
            collective_id=0, has_side_effects=True, vmem_limit_bytes=67043328
        ),
    )(
        x_rows,
        x_rows.reshape(tpn, trows, local),
        in_gain.reshape(1, local),
        query_weight,
        key_weight,
        value_weight,
        outgate_weight,
        gate,
        forget_bias.reshape(1, heads),
        state_matrix,
        state_norm,
        state_max,
        head_gain.astype(F32).reshape(heads, dv),
        out_weight,
        mix_gain.reshape(1, local),
        up_weight,
        down_weight,
    )
    return (mixed.reshape(total, local), new_matrix, new_norm, new_max)


def solution(mesh):
    placed = (
        P("grp", "kv"),
        P("kv"),
        P("kv", "tp"),
        P("kv", "tp"),
        P("kv", "tp"),
        P("kv", "tp"),
        P("kv", "tp"),
        P("kv", "tp"),
        P("tp"),
        P(("grp", "kv"), "tp", None, None),
        P(("grp", "kv"), "tp", None),
        P(("grp", "kv"), "tp"),
        P("tp"),
        P("tp", "kv"),
        P("kv"),
        P("kv", "tp"),
        P("tp", "kv"),
    )
    return jax.shard_map(
        functools.partial(per_device, mesh.shape["kv"], mesh.shape["tp"]),
        mesh=mesh,
        in_specs=placed,
        out_specs=(
            P("grp", "kv"),
            P(("grp", "kv"), "tp", None, None),
            P(("grp", "kv"), "tp", None),
            P(("grp", "kv"), "tp"),
        ),
        check_vma=False,
    )
```

time: 356 us -> 181 us (0.51)
  waiting for transfers between devices: 216 us -> 0 us
  Pallas kernels: 0 us -> 145 us
  matrix products: 47.9 us -> 0 us
  blocking collectives: 41.2 us -> 0 us
  other arithmetic: 34.2 us -> 0.9 us
  local copies, waits for them, and re-layouts: 1.59 us -> 33.7 us
  between operations: 14.8 us -> 0.66 us
    pallas_call x0 -> x1, Pallas kernels: none -> 145 us  [per_device(): pl.pallas_call(functools.partial(kernel, kvn, tpn, width, model), out_sha...]
    reduce_scatter x6 -> x0, waiting for transfers between devices: 125 us -> none  [the longest x1 31.8 us: per_device(): lax.psum_scatter(up_part, 'kv', scatter_dimension=0, tiled=True)]
    psum x2 -> x0, waiting for transfers between devices: 63 us -> none  [the longest x1 31.9 us: per_device(): branch = lax.psum(branch, 'tp')]
    dot_general x8 -> x0, matrix products: 46.1 us -> none  [the longest x1 19.8 us: per_device(): jnp.einsum('bhd,bhde->bhe', query, new_matrix, precision=lax.Precision.HI...]
    unnamed x30 -> x9, local copies, waits for them, and re-layouts: 1.58 us -> 29.9 us
    all_gather x1 -> x0, waiting for transfers between devices: 27.4 us -> none  [per_device(): lax.all_gather(hidden, 'kv', axis=0, tiled=True)]
    unnamed x2 -> x0, blocking collectives: 25.3 us -> none
    add x2 -> x0, other arithmetic: 24.6 us -> none  [the longest x1 24.5 us: per_device(): fdecay[:, :, None, None] * state_matrix]
  transfers between devices with their start and end apart: 9 -> 0, of which waited for: 8 -> 0; matrix products, arithmetic and copies ran while one was open for 5% -> 0% of each run, Pallas kernels for 0% -> 0%
where the time goes in v1:
time: 181 us; the launch traced here: 180 us
  Pallas kernels  145 us (80%)
  local copies, waits for them, and re-layouts  33.7 us (19%)
    pallas_call x1, Pallas kernels, per_device(): pl.pallas_call(functools.partial(kernel, kvn, tpn, width, model), out_sha...  145 us
    unnamed x9, local copies, waits for them, and re-layouts  29.9 us

profile of v1, /device:TPU:0, one launch (start us, length us, event | category | flops | bytes accessed | tf_op | source)
XLA Modules:
  0.0 180.4 jit_solution(14133066658705827928)
XLA Ops:
  0.6 1.3 reshape.29.gain_ref
  1.9 1.3 reshape.33.mix_gain_ref
  3.2 1.3 reshape.36.head_gain_ref
  4.5 1.4 copy.23.max_ref
  5.8 0.9 copy.21
  6.7 0.9 copy.22
  7.6 0.9 fusion.2.gate_ref
  8.5 145.1 %shard_map.192 = (bf16[4,32,1024]{2,1,0:T(8,128)(2,1)}, f32[32,8,128,256]{3,2,1,0:T(8,128)}, f32[32,8,128]{2,1,0:T(8,128)}, f32[32,8]{1,0:T(8,128)}) custom-call(bf16[128,1024]{1,0:T(8,128)(2,1)} %x_ref.1, bf16[4,32,1024]{2,1,0:T(8,128)(2,1)} %bitcast.3, bf16[1,1024]{1,0:T(2,128)(2,1)} %reshape.29.gain_ref, bf16[1024,1024]{1,0:T(8,128)(2,1)} %q_hbm.1, ...), custom_call_target="tpu_custom_call" | custom-call | tf_op jit(solution)/shard_map/pallas_call | solution.py:523
  153.6 1.4 copy.24
  155.0 1.7 copy.28
  156.7 0.0 copy-start
  156.7 23.0 %copy.29 = f32[32,8,128,256]{3,2,1,0:T(8,128)} copy(f32[32,8,128,256]{3,2,1,0:T(8,128)} %get-tuple-element.21) | data formatting | bytes 67108864
  179.7 0.0 copy-done
  179.7 0.7 copy.30
Async XLA Ops:
  156.7 23.0 %copy-start = (f32[32,8,128]{2,1,0:T(8,128)S(1)}, f32[32,8,128]{2,1,0:T(8,128)}, u32[]{:S(2)}) copy-start(f32[32,8,128]{2,1,0:T(8,128)} %get-tuple-element.22) | copy-start | bytes 393220
